TPU v7x, 32 devices: a whole 2x2x4 slice. The times are simulated.
32 devices in a mesh: kv: 8 (over z, x), tp: 4 (over y, core).
Axes of the slice: x: 2, y: 2, z: 4, core: 2. Of those that a mesh axis runs over, the one named last changes fastest.
Arguments:
- tokens: bfloat16 [4096, 2048], P('kv'), may hold values from -64 to 64
- query_weight: bfloat16 [2048, 2048], P(None, 'tp'), may hold values from -0.1875 to 0.1875
- chosen_key_weight: bfloat16 [2048, 512], P(None, 'tp'), may hold values from -0.125 to 0.125
- chosen_value_weight: bfloat16 [2048, 512], P(None, 'tp'), may hold values from -0.125 to 0.125
- summary_key_weight: bfloat16 [2048, 512], P(None, 'tp'), may hold values from -0.125 to 0.125
- summary_value_weight: bfloat16 [2048, 512], P(None, 'tp'), may hold values from -0.125 to 0.125
- squeeze_key_in: bfloat16 [2048, 128], replicated, may hold values from -0.125 to 0.125
- squeeze_key_out: bfloat16 [128, 64], replicated, may hold values from -1 to 1
- squeeze_value_in: bfloat16 [2048, 128], replicated, may hold values from -0.125 to 0.125
- squeeze_value_out: bfloat16 [128, 64], replicated, may hold values from -2 to 2
- gate_weight: bfloat16 [2, 2048, 32], P(None, None, 'tp'), may hold values from -0.125 to 0.125
- output_weight: bfloat16 [2048, 2048], P('tp'), may hold values from -1 to 1
- chosen_blocks: int32 [8, 128, 16], P('tp', 'kv'), may hold values from 0 to 127, as said below
Outputs:
- attended: bfloat16 [4096, 2048], P(('kv', 'tp'))
Inputs may be any that keep to these rules, and one draw needn't show every extreme that they name: `chosen_blocks`: each row lists 16 different blocks. The row of query block b lists b, lists b - 1 where b > 0, and lists block 0. Take the blocks at or below their query block that the rows of the query blocks of one index of kv list for one key head: at most 4 different ones lie among the positions of any other single index of kv, and exactly 4 among the positions of the first index, for every index after the first.
All inputs are finite; a program needn't handle non-finite values.
Results may differ from a plain program's by a relative error of at most 0.03.
Values may be sent and summed in bfloat16 or wider, within the bound.
A program may use at most 128 MiB of HBM per device.

v0:
```python
import jax
import jax.numpy as jnp
from jax import lax
from jax.sharding import PartitionSpec as P

HD = 64
CMP_LEN = 32
CMP_STRIDE = 16
BLK = 32


ROTARY_BASE = 10000.0
NEGATIVE_FILL = -1e30


def from_behind(block, axis, distance):
    devices = range(lax.axis_size(axis))
    route = [(i - distance, i) for i in devices if i - distance in devices]
    return lax.ppermute(block, axis, route)


def rotate(values, positions):
    halfway = values.shape[-1] // 2
    inverse = ROTARY_BASE ** (-jnp.arange(halfway, dtype=jnp.float32) / halfway)
    angles = positions.astype(jnp.float32)[:, None] * inverse[None, :]
    cosine_rows = jnp.cos(angles)[:, None, :]
    sine_rows = jnp.sin(angles)[:, None, :]
    former = values[..., :halfway]
    latter = values[..., halfway:]
    return jnp.concatenate(
        [former * cosine_rows - latter * sine_rows, latter * cosine_rows + former * sine_rows], -1
    )


def squeeze_windows(windows, weight_in, weight_out):
    total_windows = windows.shape[0]
    groups = windows.shape[2]
    head_width = windows.shape[3]
    flattened = windows.transpose(0, 2, 1, 3).reshape(total_windows * groups, CMP_LEN * head_width)
    hidden = jax.nn.gelu(jnp.dot(flattened, weight_in, preferred_element_type=jnp.float32)).astype(
        jnp.bfloat16
    )
    return jnp.dot(hidden, weight_out, preferred_element_type=jnp.float32).reshape(
        total_windows, groups, head_width
    )


def online_step(running, scores, visible, values):
    largest, summed, weighted = running
    updated = jnp.maximum(largest, jnp.max(jnp.where(visible, scores, NEGATIVE_FILL), -1))
    weights = jnp.where(visible, jnp.exp(scores - updated[..., None]), 0.0)
    shrink = jnp.exp(largest - updated)
    summed = summed * shrink + jnp.sum(weights, -1)
    weighted = weighted * shrink[..., None] + jnp.einsum(
        "grqk,kgd->grqd", weights.astype(jnp.bfloat16), values, preferred_element_type=jnp.float32
    )
    return (updated, summed, weighted)


def on_device(
    tokens,
    query_weight,
    chosen_key_weight,
    chosen_value_weight,
    summary_key_weight,
    summary_value_weight,
    squeeze_key_in,
    squeeze_key_out,
    squeeze_value_in,
    squeeze_value_out,
    gate_weight,
    output_weight,
    chosen_blocks,
):
    tok_rows = tokens.shape[0]
    heads_here = query_weight.shape[1] // HD
    groups_here = chosen_key_weight.shape[1] // HD
    per_group = heads_here // groups_here
    kv_rank = lax.axis_index("kv")
    offset = kv_rank * tok_rows
    positions = offset + jnp.arange(tok_rows, dtype=jnp.int32)
    queries = rotate(
        jnp.dot(tokens, query_weight, preferred_element_type=jnp.float32).reshape(
            tok_rows, heads_here, HD
        ),
        positions,
    )
    queries = queries.astype(jnp.bfloat16).reshape(tok_rows, groups_here, per_group, HD)
    chosen_keys = rotate(
        jnp.dot(tokens, chosen_key_weight, preferred_element_type=jnp.float32).reshape(
            tok_rows, groups_here, HD
        ),
        positions,
    ).astype(jnp.bfloat16)
    chosen_values = (
        jnp.dot(tokens, chosen_value_weight, preferred_element_type=jnp.float32)
        .astype(jnp.bfloat16)
        .reshape(tok_rows, groups_here, HD)
    )
    chosen_pairs = jnp.concatenate([chosen_keys, chosen_values], -1)
    raw_keys = (
        jnp.dot(tokens, summary_key_weight, preferred_element_type=jnp.float32)
        .astype(jnp.bfloat16)
        .reshape(tok_rows, groups_here, HD)
    )
    raw_values = (
        jnp.dot(tokens, summary_value_weight, preferred_element_type=jnp.float32)
        .astype(jnp.bfloat16)
        .reshape(tok_rows, groups_here, HD)
    )
    raw_pairs = jnp.concatenate([raw_keys, raw_values], -1)
    following = from_behind(raw_pairs[:CMP_STRIDE], "kv", -1)
    extended = jnp.concatenate([raw_pairs, following], 0)
    summary_count = tok_rows // CMP_STRIDE
    segments = extended.reshape(summary_count + 1, CMP_STRIDE, groups_here, 2 * HD)
    windows = jnp.concatenate([segments[:-1], segments[1:]], 1)
    summary_ends = (
        (kv_rank * summary_count + jnp.arange(summary_count, dtype=jnp.int32)) * CMP_STRIDE
        + CMP_LEN
        - 1
    )
    summary_keys = rotate(
        squeeze_windows(windows[..., :HD], squeeze_key_in, squeeze_key_out), summary_ends
    ).astype(jnp.bfloat16)
    summary_values = squeeze_windows(windows[..., HD:], squeeze_value_in, squeeze_value_out).astype(
        jnp.bfloat16
    )
    summaries = jnp.concatenate([summary_keys, summary_values], -1)
    scaling = HD ** (-0.5)
    starting = (
        jnp.full((groups_here, per_group, tok_rows), NEGATIVE_FILL, jnp.float32),
        jnp.zeros((groups_here, per_group, tok_rows), jnp.float32),
        jnp.zeros((groups_here, per_group, tok_rows, HD), jnp.float32),
    )
    portion = lax.all_gather(summaries, "kv", axis=0, tiled=True)
    length = portion.shape[0]
    ends = jnp.arange(length, dtype=jnp.int32) * CMP_STRIDE + CMP_LEN - 1
    scores = (
        jnp.einsum("qgrd,kgd->grqk", queries, portion[..., :HD], preferred_element_type=jnp.float32)
        * scaling
    )
    visible = (ends[None, :] <= positions[:, None])[None, None]
    folded = online_step(starting, scores, visible, portion[..., HD:])
    compressed = folded[2] / jnp.maximum(folded[1], 1.0)[..., None]
    block_count = tok_rows // BLK

    def span_step(running, stretch, leading):
        length = stretch.shape[0]
        key_positions = leading + jnp.arange(length, dtype=jnp.int32)
        listed = jnp.any(
            chosen_blocks[:, :, :, None] == (key_positions // BLK)[None, None, None, :], axis=2
        )
        listed = jnp.broadcast_to(
            listed[:, :, None, :], (groups_here, block_count, BLK, length)
        ).reshape(groups_here, tok_rows, length)
        visible = (listed & (key_positions[None, None, :] <= positions[None, :, None]))[:, None]
        scores = (
            jnp.einsum(
                "qgrd,kgd->grqk", queries, stretch[..., :HD], preferred_element_type=jnp.float32
            )
            * scaling
        )
        return online_step(running, scores, visible, stretch[..., HD:])

    def maybe_step(running, stretch, leading):

        def step_taken(carried):
            return span_step(carried, stretch, leading)

        def step_skipped(carried):
            return carried

        return lax.cond(leading <= offset + tok_rows - 1, step_taken, step_skipped, running)

    portion = lax.all_gather(chosen_pairs, "kv", axis=0, tiled=True)
    length = portion.shape[0]
    stretch_rows = tok_rows * 4

    def visit_span(number, carried):
        stretch = lax.dynamic_slice_in_dim(portion, number * stretch_rows, stretch_rows, 0)
        return maybe_step(carried, stretch, number * stretch_rows)

    folded_chosen = lax.fori_loop(0, length // stretch_rows, visit_span, starting)
    selected = folded_chosen[2] / folded_chosen[1][..., None]
    first_gates = jax.nn.sigmoid(
        jnp.dot(tokens, gate_weight[0], preferred_element_type=jnp.float32)
    )
    second_gates = jax.nn.sigmoid(
        jnp.dot(tokens, gate_weight[1], preferred_element_type=jnp.float32)
    )
    first_gates = first_gates.reshape(tok_rows, groups_here, per_group).transpose(1, 2, 0)[
        ..., None
    ]
    second_gates = second_gates.reshape(tok_rows, groups_here, per_group).transpose(1, 2, 0)[
        ..., None
    ]
    blended = (
        (first_gates * compressed + second_gates * selected)
        .transpose(2, 0, 1, 3)
        .reshape(tok_rows, heads_here * HD)
        .astype(jnp.bfloat16)
    )
    attended = lax.psum_scatter(
        jnp.dot(blended, output_weight, preferred_element_type=jnp.float32).astype(jnp.bfloat16),
        "tp",
        scatter_dimension=0,
        tiled=True,
    )
    return attended


def solution(mesh):
    return jax.shard_map(
        on_device,
        mesh=mesh,
        in_specs=(
            P("kv", None),
            P(None, "tp"),
            P(None, "tp"),
            P(None, "tp"),
            P(None, "tp"),
            P(None, "tp"),
            P(),
            P(),
            P(),
            P(),
            P(None, None, "tp"),
            P("tp", None),
            P("tp", "kv", None),
        ),
        out_specs=P(("kv", "tp"), None),
        check_vma=False,
    )
```

profile of v0, /device:TPU:26, one launch (start us, length us, event | category | flops | bytes accessed | tf_op | source)
XLA Modules:
  0.0 238.9 jit_solution(17851520680205878891)
XLA Ops:
  6.6 2.7 %convolution_convert_fusion.1 = bf16[512,128]{0,1:T(8,128)(2,1)S(1)} fusion(bf16[512,2048]{1,0:T(8,128)(2,1)} %param.17, bf16[2048,128]{1,0:T(8,128)(2,1)} %param.20), kind=kOutput, calls=%fused_computation.44 | convolution fusion | flops 268500992 | bytes 2752512 | tf_op jit(solution)/shard_map/dot_general | solution.py:96
  9.2 2.5 %fusion.91 = f32[512,128]{0,1:T(8,128)S(1)} fusion(bf16[512,2048]{1,0:T(8,128)(2,1)} %param.17, bf16[2048,128]{1,0:T(8,128)(2,1)} %param.19), kind=kOutput, calls=%fused_computation.133 | convolution fusion | flops 268435456 | bytes 2883584 | tf_op jit(solution)/shard_map/dot_general | solution.py:90
  11.7 0.3 multiply_cosine_fusion
  12.1 0.7 pad_maximum_fusion.4
  12.9 2.4 %convolution_convert_fusion.2 = bf16[512,128]{0,1:T(8,128)(2,1)S(1)} fusion(bf16[512,2048]{1,0:T(8,128)(2,1)} %param.17, bf16[2048,128]{1,0:T(8,128)(2,1)S(1)} %copy-done.7), kind=kOutput, calls=%fused_computation.45 | convolution fusion | flops 268500992 | bytes 2752512 | tf_op jit(solution)/shard_map/dot_general | solution.py:107
  15.3 0.2 copy.53
  15.5 2.5 %convolution_convert_fusion.3 = bf16[512,128]{0,1:T(8,128)(2,1)S(1)} fusion(bf16[512,2048]{1,0:T(8,128)(2,1)} %param.17, bf16[2048,128]{1,0:T(8,128)(2,1)} %param.21), kind=kOutput, calls=%fused_computation.46 | convolution fusion | flops 268500992 | bytes 2752512 | tf_op jit(solution)/shard_map/dot_general | solution.py:102
  18.0 0.2 copy.52
  18.2 0.7 pad_maximum_fusion.6
  18.9 3.0 %collective-permute-start = (bf16[16,2,128]{2,0,1:T(8,128)(2,1)}, bf16[16,2,128]{2,0,1:T(8,128)(2,1)}, u32[]{:S(2)}, u32[]{:S(2)}) collective-permute-start(bf16[16,2,128]{2,0,1:T(8,128)(2,1)} %pad_maximum_fusion.6), channel_id=1, source_target_pairs={{4,0},{8,4},{12,8},{16,12},{20,16},{24,20},{28,24},{5,1},{9,5},{13... | collective-permute-start | bytes 24584 | tf_op jit(solution)/shard_map/ppermute | solution.py:19
  21.9 3.6 %fusion.90 = f32[512,512]{0,1:T(8,128)S(1)} fusion(bf16[512,2048]{1,0:T(8,128)(2,1)} %param.17, bf16[2048,512]{1,0:T(8,128)(2,1)} %param.18), kind=kOutput, calls=%fused_computation.132 | convolution fusion | flops 1073741824 | bytes 5242880 | tf_op jit(solution)/shard_map/dot_general | solution.py:83
  25.5 0.2 subtract_convert_fusion
  25.7 0.1 broadcast_compare_fusion.1
  25.9 0.7 multiply_cosine_fusion.1
  26.6 2.9 %fusion.34 = f32[512,8]{0,1:T(8,128)} fusion(bf16[512,2048]{1,0:T(8,128)(2,1)} %param.17, bf16[2,2048,8]{1,2,0:T(8,128)(2,1)} %param.27), kind=kOutput, calls=%fused_computation.51 | convolution fusion | flops 16789504 | bytes 2146304 | tf_op jit(solution)/shard_map/dot_general | solution.py:189
  29.5 2.3 fusion.37
  31.8 0.8 pad_maximum_fusion.1
  32.6 0.8 copy.51
  33.4 0.7 copy.50
  34.1 1.0 concatenate.38
  35.2 1.0 concatenate.37
  36.2 1.3 reshape.285
  37.5 0.6 reshape.278
  38.2 0.8 pad_maximum_fusion.2
  39.0 0.3 copy.54
  39.3 1.0 pad_maximum_fusion
  40.3 1.0 slice_bitcast_fusion.1
  41.3 0.1 copy.56
  41.4 0.5 reshape.283
  41.9 0.1 copy.55
  42.0 0.5 reshape.281
  42.5 1.4 fusion.64
  43.9 0.8 subtract_convert_fusion.2
  44.7 1.4 convolution_convert_fusion.4
  46.1 0.1 pad_maximum_fusion.5
  46.3 31.1 %all_gather.6 = bf16[256,2,128]{2,1,0:T(2,128)(2,1)S(1)} all-gather(bf16[32,2,128]{2,1,0:T(2,128)(2,1)S(1)} %pad_maximum_fusion.5), channel_id=1, replica_groups=mesh['kv'=8,'tp'=4] {'kv'}, dimensions={0}, use_global_device_ids=true | all-gather | bytes 147456 | tf_op jit(solution)/shard_map/all_gather | solution.py:135
  77.3 0.2 fusion.85
  77.6 0.1 copy.66
  77.7 0.7 copy.67
  78.4 1.9 fusion.21
  80.3 2.0 copy-done.2
  82.4 0.9 fusion.24
  83.3 0.6 exponential_multiply_fusion
  83.9 0.1 broadcast_in_dim.93
  84.1 109.8 %while.20 = (s32[]{:T(128)}, f32[2,4,512]{2,1,0:T(4,128)S(1)}, f32[2,4,512]{2,1,0:T(4,128)S(1)}, f32[2,4,512,64]{2,3,1,0:T(8,128)S(1)}, s32[]{:T(128)}, /*index=...) while((s32[]{:T(128)}, f32[2,4,512]{2,1,0:T(4,128)S(1)}, ...), condition=%wide.region_8.9_spmd.clone, body=%wide.region_2.8_spmd.clone.sunk | while | flops 2245501440 | bytes 127838584 | solution.py:183
  84.1 54.9 %conditional.3 = ((f32[2,4,512]{2,1,0:T(4,128)S(1)}, f32[2,4,512]{2,1,0:T(4,128)S(1)}, f32[2,4,512,64]{2,3,1,0:T(8,128)S(1)})) conditional(s32[]{:T(128)} %convert_element_type.107, (f32[2,4,512]{2,1,0:T(4,128)S(1)}, f32[2,4,512]{2,1,0:T(4,128)S(1)}, f32[2,4,512,64]{2,3,1,0:T(8,128)S(1)}) %tuple.69, (s32[2,16,16]{2,1,0:T(8,128)S(1)}, s32[]{:T(128)}, ...), branch_computations={%region_3.3_spmd, %region_4.7_spmd} | conditional | flops 2245501440 | bytes 127836296 | solution.py:173
  84.2 0.7 broadcast_compare_fusion
  84.8 1.0 compare_reduce_fusion
  85.9 2.6 %bitcast_and_fusion = pred[2,512,2048]{2,1,0:T(8,128)(4,1)} fusion(pred[512,2048]{1,0:T(8,128)(4,1)S(1)} %broadcast_compare_fusion, pred[2,16,2048]{2,1,0:T(8,128)(4,1)S(1)} %compare_reduce_fusion), kind=kLoop, calls=%fused_computation.10 | loop fusion | flops 2097152 | bytes 3211264 | tf_op jit(solution)/shard_map/while/body/eval_jaxpr/cond/branch_1_fun/and | solution.py:156
  88.5 6.1 %copy.48 = pred[2,512,2048]{1,2,0:T(8,128)(4,1)} copy(pred[2,512,2048]{2,1,0:T(8,128)(4,1)} %bitcast_and_fusion) | data formatting | bytes 4194304 | tf_op jit(solution)/shard_map/while/body/eval_jaxpr/cond/branch_1_fun/and | solution.py:156
  94.6 15.2 %fusion.2 = (f32[2,4,512]{2,1,0:T(4,128)S(1)}, f32[2,2048,512,4]{2,1,3,0:T(8,128)}) fusion(pred[2,512,2048]{1,2,0:T(8,128)(4,1)} %copy.48, bf16[512,2,4,64]{0,3,2,1:T(8,128)(2,1)} %get-tuple-element.301, bf16[4096,2,128]{0,2,1:T(8,128)(2,1)} %get-tuple-element.300, s32[]{:T(128)S(6)} %select_n.35), kind=kOutput, calls=%fused_computation.3 | convolution fusion | flops 1098903552 | bytes 36716548 | tf_op jit(solution)/shard_map/while/body/eval_jaxpr/cond/branch_1_fun/qgrd,kgd->grqk/dot_general | solution.py:158
  109.8 14.3 %fusion.6 = f32[2,4,512]{2,1,0:T(4,128)S(1)} fusion(f32[2,2048,512,4]{2,1,3,0:T(8,128)} %get-tuple-element.369, f32[2,4,512]{2,1,0:T(4,128)S(1)} %max.12, pred[2,512,2048]{1,2,0:T(8,128)(4,1)S(1)} %copy-done.1), kind=kLoop, calls=%fused_computation.7 | loop fusion | flops 33550336 | bytes 35684352 | tf_op jit(solution)/shard_map/while/body/eval_jaxpr/cond/branch_1_fun/reduce_sum | solution.py:53
  124.2 14.9 %fusion.10 = f32[2,4,512,64]{2,3,1,0:T(8,128)S(1)} fusion(f32[2,2048,512,4]{2,1,3,0:T(8,128)} %get-tuple-element.369, f32[2,4,512]{2,1,0:T(4,128)S(1)} %max.12, pred[2,512,2048]{1,2,0:T(8,128)(4,1)} %copy.48, f32[2,4,512,64]{2,3,1,0:T(8,128)S(1)} %get-tuple-element.303, bf16[4096,2,128]{0,2,1:T(8,128)(2,1)} %get-tuple-element.300, s32[]{:T(128)S(6)} %select_n.35, ...), kind=kOutput, calls=%fused_computation.13 | convolution fusion | flops 1107820544 | bytes 38305800 | tf_op jit(solution)/shard_map/while/body/eval_jaxpr/cond/branch_1_fun/grqk,kgd->grqd/dot_general | solution.py:54
  139.1 54.8 %conditional.3 = ((f32[2,4,512]{2,1,0:T(4,128)S(1)}, f32[2,4,512]{2,1,0:T(4,128)S(1)}, f32[2,4,512,64]{2,3,1,0:T(8,128)S(1)})) conditional(s32[]{:T(128)} %convert_element_type.107, (f32[2,4,512]{2,1,0:T(4,128)S(1)}, f32[2,4,512]{2,1,0:T(4,128)S(1)}, f32[2,4,512,64]{2,3,1,0:T(8,128)S(1)}) %tuple.69, (s32[2,16,16]{2,1,0:T(8,128)S(1)}, s32[]{:T(128)}, ...), branch_computations={%region_3.3_spmd, %region_4.7_spmd} | conditional | flops 2245501440 | bytes 127836296 | solution.py:173
  139.1 0.7 broadcast_compare_fusion
  139.8 1.0 compare_reduce_fusion
  140.8 2.6 %bitcast_and_fusion = pred[2,512,2048]{2,1,0:T(8,128)(4,1)} fusion(pred[512,2048]{1,0:T(8,128)(4,1)S(1)} %broadcast_compare_fusion, pred[2,16,2048]{2,1,0:T(8,128)(4,1)S(1)} %compare_reduce_fusion), kind=kLoop, calls=%fused_computation.10 | loop fusion | flops 2097152 | bytes 3211264 | tf_op jit(solution)/shard_map/while/body/eval_jaxpr/cond/branch_1_fun/and | solution.py:156
  143.5 6.1 %copy.48 = pred[2,512,2048]{1,2,0:T(8,128)(4,1)} copy(pred[2,512,2048]{2,1,0:T(8,128)(4,1)} %bitcast_and_fusion) | data formatting | bytes 4194304 | tf_op jit(solution)/shard_map/while/body/eval_jaxpr/cond/branch_1_fun/and | solution.py:156
  149.5 15.2 %fusion.2 = (f32[2,4,512]{2,1,0:T(4,128)S(1)}, f32[2,2048,512,4]{2,1,3,0:T(8,128)}) fusion(pred[2,512,2048]{1,2,0:T(8,128)(4,1)} %copy.48, bf16[512,2,4,64]{0,3,2,1:T(8,128)(2,1)} %get-tuple-element.301, bf16[4096,2,128]{0,2,1:T(8,128)(2,1)} %get-tuple-element.300, s32[]{:T(128)S(6)} %select_n.35), kind=kOutput, calls=%fused_computation.3 | convolution fusion | flops 1098903552 | bytes 36716548 | tf_op jit(solution)/shard_map/while/body/eval_jaxpr/cond/branch_1_fun/qgrd,kgd->grqk/dot_general | solution.py:158
  164.8 14.3 %fusion.6 = f32[2,4,512]{2,1,0:T(4,128)S(1)} fusion(f32[2,2048,512,4]{2,1,3,0:T(8,128)} %get-tuple-element.369, f32[2,4,512]{2,1,0:T(4,128)S(1)} %max.12, pred[2,512,2048]{1,2,0:T(8,128)(4,1)S(1)} %copy-done.1), kind=kLoop, calls=%fused_computation.7 | loop fusion | flops 33550336 | bytes 35684352 | tf_op jit(solution)/shard_map/while/body/eval_jaxpr/cond/branch_1_fun/reduce_sum | solution.py:53
  179.1 14.8 %fusion.10 = f32[2,4,512,64]{2,3,1,0:T(8,128)S(1)} fusion(f32[2,2048,512,4]{2,1,3,0:T(8,128)} %get-tuple-element.369, f32[2,4,512]{2,1,0:T(4,128)S(1)} %max.12, pred[2,512,2048]{1,2,0:T(8,128)(4,1)} %copy.48, f32[2,4,512,64]{2,3,1,0:T(8,128)S(1)} %get-tuple-element.303, bf16[4096,2,128]{0,2,1:T(8,128)(2,1)} %get-tuple-element.300, s32[]{:T(128)S(6)} %select_n.35, ...), kind=kOutput, calls=%fused_computation.13 | convolution fusion | flops 1107820544 | bytes 38305800 | tf_op jit(solution)/shard_map/while/body/eval_jaxpr/cond/branch_1_fun/grqk,kgd->grqd/dot_general | solution.py:54
  194.0 3.3 %add_convert_fusion = bf16[2,4,512,64]{2,3,1,0:T(8,128)(2,1)S(1)} fusion(f32[2,4,512,64]{2,3,1,0:T(8,128)S(1)} %get-tuple-element.319, f32[2,256,512,4]{2,1,3,0:T(8,128)} %copy-done.2, f32[2,4,512]{2,1,0:T(4,128)} %copy-done.9, pred[512,256]{0,1:T(8,128)(4,1)S(1)} %copy-done.6, f32[2,4,512]{2,1,0:T(4,128)S(1)} %get-tuple-element.320, ...), kind=kOutput, calls=%fused_computation.56 | convolution fusion | flops 140247040 | bytes 6062080 | tf_op jit(solution)/shard_map/grqk,kgd->grqd/dot_general | solution.py:54
  197.2 2.6 %convolution_convert_fusion = bf16[512,2048]{1,0:T(8,128)(2,1)} fusion(bf16[512,512]{0,1:T(8,128)(2,1)S(1)} %bitcast.140, bf16[512,2048]{1,0:T(8,128)(2,1)S(1)} %copy-done), kind=kOutput, calls=%fused_computation.40 | convolution fusion | flops 1074790400 | bytes 4718592 | tf_op jit(solution)/shard_map/dot_general | solution.py:204
  199.9 32.2 %reduce-scatter.2.cloned.1.call-done = bf16[128,2048]{1,0:T(8,128)(2,1)} async-done(((bf16[512,2048]{1,0:T(8,128)(2,1)}), bf16[128,2048]{1,0:T(8,128)(2,1)}) %reduce-scatter.2.cloned.1.call-update) | async-done | bytes 524304 | tf_op jit(solution)/shard_map/reduce_scatter | solution.py:203
  (60 shorter events, 0.3 us)
Async XLA Ops:
  6.5 190.7 %copy-start = (bf16[512,2048]{1,0:T(8,128)(2,1)S(1)}, bf16[512,2048]{1,0:T(8,128)(2,1)}, u32[]{:S(2)}) copy-start(bf16[512,2048]{1,0:T(8,128)(2,1)} %param.28) | copy-start | bytes 6291460
  6.5 6.4 %copy-start.7 = (bf16[2048,128]{1,0:T(8,128)(2,1)S(1)}, bf16[2048,128]{1,0:T(8,128)(2,1)}, u32[]{:S(2)}) copy-start(bf16[2048,128]{1,0:T(8,128)(2,1)} %param.22) | copy-start | bytes 1572868
  6.5 77.3 %all-gather.2.cloned.1.call-start = ((), (), s32[]{:S(2)}) async-start(), calls=%async_computation.1 | async-start | bytes 2359296 | tf_op jit(solution)/shard_map/all_gather | solution.py:175
  12.8 219.3 %reduce-scatter.2.cloned.1.call-start = ((), (), s32[]{:S(2)}) async-start(), calls=%async_computation.2 | async-start | bytes 2621440 | tf_op jit(solution)/shard_map/reduce_scatter | solution.py:203
  18.9 19.3 %collective-permute-start = (bf16[16,2,128]{2,0,1:T(8,128)(2,1)}, bf16[16,2,128]{2,0,1:T(8,128)(2,1)}, u32[]{:S(2)}, u32[]{:S(2)}) collective-permute-start(bf16[16,2,128]{2,0,1:T(8,128)(2,1)} %pad_maximum_fusion.6), channel_id=1, source_target_pairs={{4,0},{8,4},{12,8},{16,12},{20,16},{24,20},{28,24},{5,1},{9,5},{13... | collective-permute-start | bytes 24584 | tf_op jit(solution)/shard_map/ppermute | solution.py:19
  25.7 8.4 %copy-start.3 = (bf16[512,8,32]{0,2,1:T(8,128)(2,1)}, bf16[512,8,32]{0,2,1:T(8,128)(2,1)S(1)}, u32[]{:S(2)}) copy-start(bf16[512,8,32]{0,2,1:T(8,128)(2,1)S(1)} %get-tuple-element.372) | copy-start | bytes 786436
  25.7 14.6 %copy-start.4 = (bf16[512,8,32]{0,2,1:T(8,128)(2,1)}, bf16[512,8,32]{0,2,1:T(8,128)(2,1)S(1)}, u32[]{:S(2)}) copy-start(bf16[512,8,32]{0,2,1:T(8,128)(2,1)S(1)} %get-tuple-element.373) | copy-start | bytes 786436
  25.9 54.5 %copy-start.5 = (pred[512,256]{0,1:T(8,128)(4,1)}, pred[512,256]{0,1:T(8,128)(4,1)S(1)}, u32[]{:S(2)}) copy-start(pred[512,256]{0,1:T(8,128)(4,1)S(1)} %broadcast_compare_fusion.1) | copy-start | bytes 393220
  39.0 4.9 %copy-start.11 = (f32[32,32]{1,0:T(8,128)S(1)}, f32[32,32]{1,0:T(8,128)}, u32[]{:S(2)}) copy-start(f32[32,32]{1,0:T(8,128)} %get-tuple-element.386) | copy-start | bytes 12292
  78.4 5.6 %copy-start.8 = (s32[2,16,16]{2,1,0:T(8,128)S(1)}, s32[2,16,16]{2,1,0:T(8,128)}, u32[]{:S(2)}) copy-start(s32[2,16,16]{2,1,0:T(8,128)} %param.29) | copy-start | bytes 6148
  80.3 2.1 copy-start.2
  80.3 3.8 %copy-start.9 = (f32[2,4,512]{2,1,0:T(4,128)}, f32[2,4,512]{2,1,0:T(4,128)S(1)}, u32[]{:S(2)}) copy-start(f32[2,4,512]{2,1,0:T(4,128)S(1)} %broadcast_maximum_fusion) | copy-start | bytes 49156
  84.0 109.9 %copy-start.6 = (pred[512,256]{0,1:T(8,128)(4,1)S(1)}, pred[512,256]{0,1:T(8,128)(4,1)}, u32[]{:S(2)}) copy-start(pred[512,256]{0,1:T(8,128)(4,1)} %copy-done.5) | copy-start | bytes 393220
  84.0 109.9 %copy-start.10 = (bf16[256,2,64]{0,2,1:T(8,128)(2,1)S(1)}, bf16[256,2,64]{0,2,1:T(8,128)(2,1)}, u32[]{:S(2)}) copy-start(bf16[256,2,64]{0,2,1:T(8,128)(2,1)} %copy.67) | copy-start | bytes 196612
  84.0 109.9 %copy-start.12 = (f32[512,2,4]{0,2,1:T(4,128)S(1)}, f32[512,2,4]{0,2,1:T(4,128)}, u32[]{:S(2)}) copy-start(f32[512,2,4]{0,2,1:T(4,128)} %reshape.285) | copy-start | bytes 49156
  84.1 109.9 %copy-start.13 = (f32[512,2,4]{0,2,1:T(4,128)S(1)}, f32[512,2,4]{0,2,1:T(4,128)}, u32[]{:S(2)}) copy-start(f32[512,2,4]{0,2,1:T(4,128)} %reshape.278) | copy-start | bytes 49156
  84.1 109.9 %copy-start.14 = (f32[2,4,512]{2,1,0:T(4,128)S(1)}, f32[2,4,512]{2,1,0:T(4,128)}, u32[]{:S(2)}) copy-start(f32[2,4,512]{2,1,0:T(4,128)} %get-tuple-element.382) | copy-start | bytes 49156
  84.1 109.9 %copy-start.15 = (f32[2,4,512]{2,1,0:T(4,128)S(1)}, f32[2,4,512]{2,1,0:T(4,128)}, u32[]{:S(2)}) copy-start(f32[2,4,512]{2,1,0:T(4,128)} %get-tuple-element.383) | copy-start | bytes 49156
  94.6 15.3 %copy-start.1 = (pred[2,512,2048]{1,2,0:T(8,128)(4,1)S(1)}, pred[2,512,2048]{1,2,0:T(8,128)(4,1)}, u32[]{:S(2)}) copy-start(pred[2,512,2048]{1,2,0:T(8,128)(4,1)} %copy.48) | copy-start | bytes 6291460 | tf_op jit(solution)/shard_map/while/body/eval_jaxpr/cond
  149.5 15.3 %copy-start.1 = (pred[2,512,2048]{1,2,0:T(8,128)(4,1)S(1)}, pred[2,512,2048]{1,2,0:T(8,128)(4,1)}, u32[]{:S(2)}) copy-start(pred[2,512,2048]{1,2,0:T(8,128)(4,1)} %copy.48) | copy-start | bytes 6291460 | tf_op jit(solution)/shard_map/while/body/eval_jaxpr/cond
Sparse Core Ops, SparseCore 0:
  13.0 49.2 all-gather.1
  200.0 32.0 reduce-scatter.1
where the time goes:
time: 242 us; the launch traced here: 239 us
  matrix products  89.5 us (37%)
  other arithmetic  45.3 us (19%)
  waiting for transfers between devices  32.3 us (13%)
  blocking collectives  31.1 us (13%)
  local copies, waits for them, and re-layouts  23.7 us (10%)
  between operations  13.8 us (6%)
  starting transfers between devices  3.07 us (1%)
    dot_general x3, matrix products, online_step(): jnp.einsum('grqk,kgd->grqd', weights.astype(jnp.bfloat16), values, prefer...  32.9 us
    reduce_scatter x1, waiting for transfers between devices, on_device(): lax.psum_scatter(jnp.dot(blended, output_weight, preferred_element_type=j...  32.2 us
    all_gather x1, blocking collectives, on_device(): portion = lax.all_gather(summaries, 'kv', axis=0, tiled=True)  31.1 us
    dot_general x2, matrix products, span_step(): jnp.einsum('qgrd,kgd->grqk', queries, stretch[..., :HD], preferred_elemen...  30.5 us
    reduce_sum x3, other arithmetic, online_step(): summed = summed * shrink + jnp.sum(weights, -1)  29.5 us
    and x2, local copies, waits for them, and re-layouts, span_step(): listed & (key_positions[None, None, :] <= positions[None, :, None])  12.1 us
    and x2, other arithmetic, span_step(): listed & (key_positions[None, None, :] <= positions[None, :, None])  5.25 us
  transfers between devices with their start and end apart: 3, of which 1 were waited for; matrix products, arithmetic and copies ran while one was open for 14% of the time, Pallas kernels for 0%

commit v1 on v0

--- a/solution.py
+++ b/solution.py
@@ -1,12 +1,19 @@
+import functools
+
+import numpy as np
 import jax
 import jax.numpy as jnp
 from jax import lax
+from jax.experimental import pallas as pl
+from jax.experimental.pallas import tpu as pltpu
 from jax.sharding import PartitionSpec as P
 
 HD = 64
 CMP_LEN = 32
 CMP_STRIDE = 16
 BLK = 32
+CAP = 4
+LANES = 128
 
 
 ROTARY_BASE = 10000.0
@@ -209,9 +216,571 @@
     return attended
 
 
+def dot(a, b):
+    return jnp.dot(a, b, preferred_element_type=jnp.float32)
+
+
+def dot_nt(a, b):
+    return lax.dot_general(a, b, (((1,), (1,)), ((), ())), preferred_element_type=jnp.float32)
+
+
+def low_half(shape):
+    return lax.broadcasted_iota(jnp.int32, shape, 1) < HD
+
+
+def turn(x, cos, sin):
+    quarter = HD // 2
+    lane = lax.broadcasted_iota(jnp.int32, x.shape, 1)
+    swapped = jnp.where(
+        lane % HD < quarter, pltpu.roll(x, LANES - quarter, 1), pltpu.roll(x, quarter, 1)
+    )
+    return x * cos + swapped * sin
+
+
+def pair_halves(a, b):
+    low = low_half(a.shape)
+    return jnp.where(low, a, pltpu.roll(b, HD, 1)), jnp.where(low, pltpu.roll(a, HD, 1), b)
+
+
+def layer_kernel(
+    n,
+    groups,
+    per_group,
+    loc_ref,
+    tokens_hbm,
+    wq_hbm,
+    wck_hbm,
+    wcv_hbm,
+    wsk_hbm,
+    wsv_hbm,
+    ski_hbm,
+    svi_hbm,
+    sko_ref,
+    svo_ref,
+    gate_ref,
+    wo_hbm,
+    slots_ref,
+    keypos_ref,
+    turns_ref,
+    bases_ref,
+    sturns_ref,
+    out_ref,
+    tok,
+    wq,
+    wc,
+    ws,
+    wki,
+    wvi,
+    wo,
+    slotbuf,
+    kvc,
+    kvstage,
+    kvbuf,
+    rawf,
+    halo_out,
+    halo_in,
+    sumown,
+    sumbuf,
+    qbuf,
+    gates,
+    gath,
+    blended,
+    part_a,
+    part_b,
+    part_c,
+    got_a,
+    got_b,
+    got_c,
+    load_sem,
+    slot_send,
+    slot_recv,
+    kv_send,
+    kv_recv,
+    sum_send,
+    sum_recv,
+    halo_send,
+    halo_recv,
+    rs_send,
+    rs_recv,
+):
+    me = lax.axis_index("kv")
+    tp = lax.axis_index("tp")
+    rows = tok.shape[0]
+    blocks = rows // BLK
+    heads = groups * per_group
+    depth = tok.shape[1]
+    wide = CAP * BLK
+    own_base = n * CAP
+    summaries = rows // CMP_STRIDE
+    half = wki.shape[0]
+    partner = tp + 1 - 2 * (tp % 2)
+    across = (tp + 2) % 4
+    diagonal = partner + 2 - 4 * (partner // 2)
+
+    loads = []
+
+    def load(src, dst):
+        copy = pltpu.make_async_copy(src, dst, load_sem.at[len(loads)])
+        copy.start()
+        loads.append(copy)
+        return copy
+
+    load_c = [
+        load(tokens_hbm, tok),
+        load(wck_hbm, wc.at[:, 0:LANES]),
+        load(wcv_hbm, wc.at[:, LANES : 2 * LANES]),
+    ]
+    load_s = [
+        load(wsk_hbm, ws.at[:, 0:LANES]),
+        load(wsv_hbm, ws.at[:, LANES : 2 * LANES]),
+    ]
+    load_i = [
+        load(ski_hbm.at[0:half], wki.at[:, 0:LANES]),
+        load(ski_hbm.at[half : 2 * half], wki.at[:, LANES : 2 * LANES]),
+        load(svi_hbm.at[0:half], wvi.at[:, 0:LANES]),
+        load(svi_hbm.at[half : 2 * half], wvi.at[:, LANES : 2 * LANES]),
+    ]
+    load_q = [load(wq_hbm, wq)]
+    load_o = [load(wo_hbm, wo)]
+
+    sumbuf[...] = jnp.zeros_like(sumbuf)
+    halo_in[...] = jnp.zeros_like(halo_in)
+    halo_out[...] = jnp.zeros_like(halo_out)
+
+    barrier = pltpu.get_barrier_semaphore()
+    for d in range(1, n):
+        pl.semaphore_signal(
+            barrier, inc=1, device_id={"kv": (me + d) % n}, device_id_type=pl.DeviceIdType.MESH
+        )
+    for other in (partner, across):
+        pl.semaphore_signal(
+            barrier, inc=1, device_id={"tp": other}, device_id_type=pl.DeviceIdType.MESH
+        )
+    pl.semaphore_wait(barrier, n + 1)
+
+    def slot_copy(d, src_rank, dst_rank):
+        return pltpu.make_async_remote_copy(
+            src_ref=slots_ref,
+            dst_ref=slotbuf.at[src_rank],
+            send_sem=slot_send.at[d],
+            recv_sem=slot_recv.at[src_rank],
+            device_id={"kv": dst_rank},
+            device_id_type=pl.DeviceIdType.MESH,
+        )
+
+    def kv_copy(d, src_rank, dst_rank):
+        return pltpu.make_async_remote_copy(
+            src_ref=kvstage.at[d],
+            dst_ref=kvbuf.at[:, pl.ds(src_rank * CAP, CAP)],
+            send_sem=kv_send.at[d],
+            recv_sem=kv_recv.at[src_rank],
+            device_id={"kv": dst_rank},
+            device_id_type=pl.DeviceIdType.MESH,
+        )
+
+    def sum_copy(d, src_rank, dst_rank):
+        return pltpu.make_async_remote_copy(
+            src_ref=sumown,
+            dst_ref=sumbuf.at[:, pl.ds(src_rank * summaries, summaries), :],
+            send_sem=sum_send.at[d],
+            recv_sem=sum_recv.at[src_rank],
+            device_id={"kv": dst_rank},
+            device_id_type=pl.DeviceIdType.MESH,
+        )
+
+    def halo_copy(dst_rank):
+        return pltpu.make_async_remote_copy(
+            src_ref=halo_out,
+            dst_ref=halo_in,
+            send_sem=halo_send,
+            recv_sem=halo_recv,
+            device_id={"kv": dst_rank},
+            device_id_type=pl.DeviceIdType.MESH,
+        )
+
+    def rs_copy(k, src, dst, target):
+        return pltpu.make_async_remote_copy(
+            src_ref=src,
+            dst_ref=dst,
+            send_sem=rs_send.at[k],
+            recv_sem=rs_recv.at[k],
+            device_id={"tp": target},
+            device_id_type=pl.DeviceIdType.MESH,
+        )
+
+    for d in range(1, n):
+
+        @pl.when(me - d >= 0)
+        def _(d=d):
+            slot_copy(d, me, me - d).start()
+
+    base_cos = bases_ref[me, 0:1, :]
+    base_sin = bases_ref[me, 1:2, :]
+    sign = jnp.where(
+        lax.broadcasted_iota(jnp.int32, (1, LANES), 1) % HD < HD // 2, -1.0, 1.0
+    )
+
+    def tables(first, count):
+        c = turns_ref[0, first : first + count, :]
+        s = turns_ref[1, first : first + count, :]
+        return c * base_cos - s * base_sin, (s * base_cos + c * base_sin) * sign
+
+    for copy in load_c:
+        copy.wait()
+    step = 128
+    for first in range(0, rows, step):
+        both = dot(tok[first : first + step, :], wc[...])
+        cos, sin = tables(first, step)
+        keys = turn(both[:, 0:LANES], cos, sin)
+        pairs = pair_halves(keys, both[:, LANES : 2 * LANES])
+        for g in range(groups):
+            pair = pairs[g].astype(jnp.bfloat16)
+            kvc[g, first : first + step, :] = pair
+            for k in range(step // BLK):
+                kvbuf[g, own_base + first // BLK + k] = pair[k * BLK : (k + 1) * BLK, :]
+
+    j = lax.broadcasted_iota(jnp.int32, (n * blocks, rows), 0)
+    c = lax.broadcasted_iota(jnp.int32, (n * blocks, rows), 1)
+    expand = jnp.where(j == me * blocks + c // BLK, 1.0, 0.0).astype(jnp.bfloat16)
+    row = lax.broadcasted_iota(jnp.int32, (wide, rows), 0)
+    col = lax.broadcasted_iota(jnp.int32, (wide, rows), 1)
+    same_place = row % BLK == col % BLK
+    row_slot = (row // BLK).astype(jnp.float32)
+    for d in range(n - 1, 0, -1):
+
+        @pl.when(me + d < n)
+        def _(d=d):
+            slot_copy(d, me + d, me).wait_recv()
+            asked = dot(slotbuf[me + d].astype(jnp.bfloat16), expand)
+            for g in range(groups):
+                pick = jnp.where(same_place & (asked[g : g + 1, :] == row_slot), 1.0, 0.0)
+                packed = dot(pick.astype(jnp.bfloat16), kvc[g]).astype(jnp.bfloat16)
+                for k in range(CAP):
+                    kvstage[d, g, k] = packed[k * BLK : (k + 1) * BLK, :]
+            kv_copy(d, me, me + d).start()
+
+    for copy in load_s:
+        copy.wait()
+    for first in range(0, rows, step):
+        both = dot(tok[first : first + step, :], ws[...])
+        rounded = both.astype(jnp.bfloat16).astype(jnp.float32)
+        for kind in range(2):
+            rawf[kind, first : first + step, :] = rounded[:, kind * LANES : (kind + 1) * LANES]
+    for copy in load_i:
+        copy.wait()
+    layers = []
+    for kind, weight in ((0, wki), (1, wvi)):
+        pieces = [[] for _ in range(groups)]
+        for p in range(0, CMP_STRIDE, 2):
+            one = rawf[kind, pl.ds(p, summaries, stride=CMP_STRIDE), :]
+            two = rawf[kind, pl.ds(p + 1, summaries, stride=CMP_STRIDE), :]
+            for g, piece in enumerate(pair_halves(one, two)):
+                pieces[g].append(piece.astype(jnp.bfloat16))
+        segments = jnp.concatenate([jnp.concatenate(pieces[g], 1) for g in range(groups)], 0)
+        layers.append(dot(segments, weight[...]))
+    for kind in range(2):
+        for g in range(groups):
+            at = kind * groups + g
+            halo_out[at : at + 1, :] = layers[kind][
+                g * summaries : g * summaries + 1, LANES : 2 * LANES
+            ]
+
+    @pl.when(me > 0)
+    def _():
+        halo_copy(me - 1).start()
+
+    for copy in load_q:
+        copy.wait()
+    scaling = HD**-0.5
+    for first in range(0, rows, step):
+        projected = dot(tok[first : first + step, :], wq[...])
+        cos, sin = tables(first, step)
+        cos = cos * scaling
+        sin = sin * scaling
+        for pair in range(heads // 2):
+            turned = turn(projected[:, pair * LANES : (pair + 1) * LANES], cos, sin)
+            low = low_half(turned.shape)
+            for odd in range(2):
+                head = 2 * pair + odd
+                g, r = head // per_group, head % per_group
+                part = pltpu.roll(turned, HD, 1) if odd else turned
+                part = jnp.where(low, part, 0.0).astype(jnp.bfloat16)
+                for k in range(step // BLK):
+                    at = (first // BLK + k) * per_group * BLK + r * BLK
+                    qbuf[g, at : at + BLK, :] = part[k * BLK : (k + 1) * BLK, :]
+    gates[...] = jax.nn.sigmoid(dot_nt(tok[...], gate_ref[...]))
+
+    @pl.when(me < n - 1)
+    def _():
+        halo_copy(me).wait_recv()
+
+    hidden = []
+    last = lax.broadcasted_iota(jnp.int32, (summaries, LANES), 0) == summaries - 1
+    for kind in range(2):
+        per = []
+        for g in range(groups):
+            here = layers[kind][g * summaries : (g + 1) * summaries, :]
+            at = kind * groups + g
+            following = jnp.where(
+                last, halo_in[at : at + 1, :], pltpu.roll(here[:, LANES:], summaries - 1, 0)
+            )
+            per.append(here[:, :LANES] + following)
+        hidden.append(jax.nn.gelu(jnp.concatenate(per, 0)).astype(jnp.bfloat16))
+    summed = dot(hidden[0], sko_ref[...]) + dot(hidden[1], svo_ref[...])
+    low = low_half((summaries, LANES))
+    sc = sturns_ref[0]
+    ss = sturns_ref[1]
+    scos = jnp.where(low, sc * base_cos - ss * base_sin, 1.0)
+    ssin = jnp.where(low, (ss * base_cos + sc * base_sin) * sign, 0.0)
+    for g in range(groups):
+        pair = turn(summed[g * summaries : (g + 1) * summaries, :], scos, ssin)
+        pair = pair.astype(jnp.bfloat16)
+        sumown[g] = pair
+        sumbuf[g, pl.ds(pl.multiple_of(me * summaries, summaries), summaries), :] = pair
+    for d in range(1, n):
+
+        @pl.when(me + d < n)
+        def _(d=d):
+            sum_copy(d, me, me + d).start()
+
+    for d in range(1, n):
+
+        @pl.when(me - d >= 0)
+        def _(d=d):
+            sum_copy(d, me - d, me).wait_recv()
+            kv_copy(d, me - d, me).wait_recv()
+
+    total = n * summaries
+    listed = keypos_ref.shape[1]
+    qrows = per_group * BLK
+    in_block = lax.broadcasted_iota(jnp.int32, (qrows, 1), 0) % BLK
+    ends = lax.broadcasted_iota(jnp.int32, (1, total), 1) * CMP_STRIDE + CMP_LEN - 1
+    per_chunk = blocks // 4
+
+    def mix(q, pairs, visible):
+        scores = jnp.where(visible, dot_nt(q, pairs), NEGATIVE_FILL)
+        largest = jnp.max(scores, -1, keepdims=True)
+        weights = jnp.where(visible, jnp.exp(scores - largest), 0.0)
+        total_weight = jnp.sum(weights, -1, keepdims=True)
+        return dot(weights.astype(jnp.bfloat16), pairs), total_weight
+
+    def attend(target):
+        def block(i, _):
+            b = target * per_chunk + i
+            pos = me * rows + b * BLK + in_block
+            gate = gates[pl.ds(pl.multiple_of(b * BLK, BLK), BLK), :]
+            for g in range(groups):
+                q = qbuf[g, pl.ds(pl.multiple_of(b * qrows, qrows), qrows), :]
+                for k in range(listed // BLK):
+                    where = loc_ref[g * blocks + b, k]
+                    gath[g, k * BLK : (k + 1) * BLK, :] = kvbuf[g, where]
+                compressed, csum = mix(q, sumbuf[g], ends <= pos)
+                key_positions = keypos_ref[pl.ds(g * blocks + b, 1), :]
+                selected, ssum = mix(q, gath[g], key_positions <= pos)
+                cinv = 1.0 / jnp.maximum(csum, 1.0)
+                sinv = 1.0 / ssum
+                heads_out = []
+                for r in range(per_group):
+                    part = slice(r * BLK, (r + 1) * BLK)
+                    h = g * per_group + r
+                    heads_out.append(
+                        compressed[part] * (cinv[part] * gate[:, h : h + 1])
+                        + selected[part] * (sinv[part] * gate[:, heads + h : heads + h + 1])
+                    )
+                for r in range(0, per_group, 2):
+                    joined = jnp.where(
+                        low_half((BLK, LANES)), pltpu.roll(heads_out[r], HD, 1), heads_out[r + 1]
+                    )
+                    at = (g * per_group + r) * HD
+                    blended[pl.ds(pl.multiple_of(i * BLK, BLK), BLK), at : at + LANES] = (
+                        joined.astype(jnp.bfloat16)
+                    )
+            return 0
+
+        lax.fori_loop(0, per_chunk, block, 0)
+
+    tile = 512
+    columns = wo.shape[1]
+
+    def project(dst, added):
+        for at in range(0, columns, tile):
+            piece = dot(blended[...], wo[:, at : at + tile])
+            for other in added:
+                piece = piece + other[:, at : at + tile].astype(jnp.float32)
+            dst[:, at : at + tile] = piece.astype(jnp.bfloat16)
+
+    attend(diagonal)
+    for copy in load_o:
+        copy.wait()
+    project(part_a, [])
+    send_a = rs_copy(0, part_a, got_a, partner)
+    send_a.start()
+    attend(across)
+    send_a.wait_recv()
+    project(part_b, [got_a])
+    send_b = rs_copy(1, part_b, got_b, across)
+    send_b.start()
+    attend(partner)
+    project(part_c, [])
+    send_c = rs_copy(2, part_c, got_c, partner)
+    send_c.start()
+    attend(tp)
+    send_c.wait_recv()
+    send_b.wait_recv()
+    project(out_ref, [got_c, got_b])
+
+    for copy in (send_a, send_b, send_c):
+        copy.wait_send()
+    for d in range(1, n):
+
+        @pl.when(me - d >= 0)
+        def _(d=d):
+            slot_copy(d, me, me - d).wait_send()
+
+        @pl.when(me + d < n)
+        def _(d=d):
+            kv_copy(d, me, me + d).wait_send()
+            sum_copy(d, me, me + d).wait_send()
+
+    @pl.when(me > 0)
+    def _():
+        halo_copy(me - 1).wait_send()
+
+
+def rotary_constants(rows, n):
+    inverse = ROTARY_BASE ** (-np.arange(HD // 2) / (HD // 2))
+    lanes = np.tile(inverse, LANES // (HD // 2))[None, :]
+
+    def table(positions):
+        angles = np.asarray(positions, np.float64)[:, None] * lanes
+        return np.stack([np.cos(angles), np.sin(angles)]).astype(np.float32)
+
+    local = table(np.arange(rows))
+    bases = table(np.arange(n) * rows).transpose(1, 0, 2)
+    ends = table(np.arange(rows // CMP_STRIDE) * CMP_STRIDE + CMP_LEN - 1)
+    return local, bases, ends
+
+
+def fused(n, *args):
+    (
+        tokens,
+        wq,
+        wck,
+        wcv,
+        wsk,
+        wsv,
+        ski,
+        sko,
+        svi,
+        svo,
+        gate_weight,
+        wo,
+        chosen,
+    ) = args
+    rows, depth = tokens.shape
+    groups = wck.shape[1] // HD
+    per_group = wq.shape[1] // wck.shape[1]
+    heads = groups * per_group
+    blocks = rows // BLK
+    listed = chosen.shape[2]
+    me = lax.axis_index("kv")
+    query_block = me * blocks + jnp.arange(blocks, dtype=jnp.int32)
+    every = n * blocks
+    hit = chosen[..., None] == jnp.arange(every, dtype=jnp.int32)
+    counted = hit & (chosen <= query_block[None, :, None])[..., None]
+    present = jnp.any(counted, axis=(1, 2))
+    by_shard = present.reshape(groups, n, blocks).astype(jnp.int32)
+    earlier = jnp.arange(blocks)[:, None] < jnp.arange(blocks)[None, :]
+    slot = jnp.sum(jnp.where(earlier, by_shard[..., None], 0), axis=2).reshape(groups, every)
+    slots = jnp.where(present, slot, -1).astype(jnp.float32)
+    slots = jnp.pad(slots, ((0, 8 - groups), (0, 0)), constant_values=-1.0)
+    chosen_slot = jnp.sum(jnp.where(hit, slot[:, None, None, :], 0), -1)
+    owner = chosen // blocks
+    loc = jnp.where(
+        owner == me,
+        n * CAP + chosen % blocks,
+        jnp.where(owner < me, owner * CAP + jnp.minimum(chosen_slot, CAP - 1), n * CAP),
+    ).reshape(groups * blocks, listed)
+    keypos = (
+        chosen[..., None] * BLK + jnp.arange(BLK, dtype=jnp.int32)
+    ).reshape(groups * blocks, listed * BLK)
+    gate = gate_weight.transpose(0, 2, 1).reshape(2 * heads, depth)
+    gate = jnp.pad(gate, ((0, LANES - 2 * heads), (0, 0)))
+    sko = jnp.pad(sko, ((0, 0), (0, HD)))
+    svo = jnp.pad(svo, ((0, 0), (HD, 0)))
+    local, bases, ends = rotary_constants(rows, n)
+    chunk = rows // 4
+    bf = jnp.bfloat16
+    hbm = pl.BlockSpec(memory_space=pl.ANY)
+    vmem = pl.BlockSpec(memory_space=pltpu.VMEM)
+    wide = CAP * BLK
+    summaries = rows // CMP_STRIDE
+    part = pltpu.VMEM((chunk, wo.shape[1]), bf)
+    dma = pltpu.SemaphoreType.DMA
+    return pl.pallas_call(
+        functools.partial(layer_kernel, n, groups, per_group),
+        out_shape=jax.ShapeDtypeStruct((chunk, wo.shape[1]), bf),
+        in_specs=[pl.BlockSpec(memory_space=pltpu.SMEM)]
+        + [hbm] * 8
+        + [vmem] * 3
+        + [hbm]
+        + [vmem] * 5,
+        out_specs=vmem,
+        scratch_shapes=[
+            pltpu.VMEM((rows, depth), bf),
+            pltpu.VMEM((depth, heads * HD), bf),
+            pltpu.VMEM((depth, 2 * LANES), bf),
+            pltpu.VMEM((depth, 2 * LANES), bf),
+            pltpu.VMEM((CMP_STRIDE * HD, 2 * LANES), bf),
+            pltpu.VMEM((CMP_STRIDE * HD, 2 * LANES), bf),
+            pltpu.VMEM(wo.shape, bf),
+            pltpu.VMEM((n, 8, every), jnp.float32),
+            pltpu.VMEM((groups, rows, LANES), bf),
+            pltpu.VMEM((n, groups, CAP, BLK, LANES), bf),
+            pltpu.VMEM((groups, n * CAP + blocks, BLK, LANES), bf),
+            pltpu.VMEM((2, rows, LANES), jnp.float32),
+            pltpu.VMEM((8, LANES), jnp.float32),
+            pltpu.VMEM((8, LANES), jnp.float32),
+            pltpu.VMEM((groups, summaries, LANES), bf),
+            pltpu.VMEM((groups, n * summaries, LANES), bf),
+            pltpu.VMEM((groups, rows * per_group, LANES), bf),
+            pltpu.VMEM((rows, LANES), jnp.float32),
+            pltpu.VMEM((groups, listed * BLK, LANES), bf),
+            pltpu.VMEM((chunk, heads * HD), bf),
+            part,
+            part,
+            part,
+            part,
+            part,
+            part,
+            dma((11,)),
+            dma((n,)),
+            dma((n,)),
+            dma((n,)),
+            dma((n,)),
+            dma((n,)),
+            dma((n,)),
+            dma(()),
+            dma(()),
+            dma((3,)),
+            dma((3,)),
+        ],
+        compiler_params=pltpu.CompilerParams(
+            collective_id=0, has_side_effects=True, vmem_limit_bytes=60 * 1024 * 1024
+        ),
+        name="layer",
+    )(loc, tokens, wq, wck, wcv, wsk, wsv, ski, svi, sko, svo, gate, wo, slots, keypos, local, bases, ends)
+
+
 def solution(mesh):
+    n = mesh.shape["kv"]
+
+    def one_device(*args):
+        fits = args[2].shape[1] == LANES and mesh.shape["tp"] == 4
+        return fused(n, *args) if fits else on_device(*args)
+
     return jax.shard_map(
-        on_device,
+        one_device,
         mesh=mesh,
         in_specs=(
             P("kv", None),

time: 242 us -> 61.1 us (0.25)
  matrix products: 89.5 us -> 0 us
  Pallas kernels: 0 us -> 47.4 us
  other arithmetic: 45.3 us -> 5.27 us
  waiting for transfers between devices: 32.3 us -> 0 us
  blocking collectives: 31.1 us -> 0 us
  local copies, waits for them, and re-layouts: 23.7 us -> 7.64 us
  between operations: 13.8 us -> 0.04 us
  starting transfers between devices: 3.07 us -> 0 us
    dot_general x16 -> x0, matrix products: 89.5 us -> none  [the longest x3 32.9 us: online_step(): jnp.einsum('grqk,kgd->grqd', weights.astype(jnp.bfloat16), values, prefer...]
    pallas_call x0 -> x1, Pallas kernels: none -> 47.4 us  [fused(): pl.pallas_call(functools.partial(layer_kernel, n, groups, per_group), out...]
    reduce_scatter x1 -> x0, waiting for transfers between devices: 32.2 us -> none  [on_device(): lax.psum_scatter(jnp.dot(blended, output_weight, preferred_element_type=j...]
    all_gather x1 -> x0, blocking collectives: 31.1 us -> none  [on_device(): portion = lax.all_gather(summaries, 'kv', axis=0, tiled=True)]
    reduce_sum x3 -> x2, other arithmetic: 29.5 us -> 1.55 us  [the longest x1 1.43 us: fused(): chosen_slot = jnp.sum(jnp.where(hit, slot[:, None, None, :], 0), -1)]
    and x2 -> x0, local copies, waits for them, and re-layouts: 12.1 us -> none  [span_step(): listed & (key_positions[None, None, :] <= positions[None, :, None])]
    and x2 -> x0, other arithmetic: 5.25 us -> none  [span_step(): listed & (key_positions[None, None, :] <= positions[None, :, None])]
    concatenate x6 -> x0, other arithmetic: 4.19 us -> none  [the longest x1 0.99 us: on_device(): windows = jnp.concatenate([segments[:-1], segments[1:]], 1)]
  transfers between devices with their start and end apart: 3 -> 0, of which waited for: 1 -> 0; matrix products, arithmetic and copies ran while one was open for 14% -> 0% of each run, Pallas kernels for 0% -> 0%
where the time goes in v1:
time: 61.1 us; the launch traced here: 60.4 us
  Pallas kernels  47.4 us (78%)
  local copies, waits for them, and re-layouts  7.64 us (13%)
  other arithmetic  5.27 us (9%)
    pallas_call x1, Pallas kernels, fused(): pl.pallas_call(functools.partial(layer_kernel, n, groups, per_group), out...  47.4 us
    unnamed x3, local copies, waits for them, and re-layouts  3.53 us
    pad x1, local copies, waits for them, and re-layouts, fused(): gate = jnp.pad(gate, ((0, LANES - 2 * heads), (0, 0)))  1.68 us
    reduce_sum x1, other arithmetic, fused(): chosen_slot = jnp.sum(jnp.where(hit, slot[:, None, None, :], 0), -1)  1.43 us
    mul x1, other arithmetic, fused(): chosen[..., None] * BLK + jnp.arange(BLK, dtype=jnp.int32)  1.34 us

profile of v1, /device:TPU:26, one launch (start us, length us, event | category | flops | bytes accessed | tf_op | source)
XLA Modules:
  0.0 60.4 jit_solution(16694347415429325656)
XLA Ops:
  0.0 0.8 %broadcast_compare_fusion = pred[2,16,16]{2,1,0:T(8,128)(4,1)S(1)} fusion(s32[2,16,16]{2,1,0:T(8,128)} %param.28, s32[16]{0:T(128)S(1)} %iota_add_fusion), kind=kLoop, calls=%fused_computation.15 | loop fusion | flops 512 | bytes 2624 | tf_op jit(solution)/shard_map/le | solution.py:690
  0.8 0.9 %fusion.1 = pred[2,128]{1,0:T(4,128)(4,1)S(1)} fusion(s32[2,16,16]{2,1,0:T(8,128)} %param.28, pred[2,16,16]{2,1,0:T(8,128)(4,1)S(1)} %broadcast_compare_fusion), kind=kLoop, calls=%fused_computation.3 | loop fusion | flops 196352 | bytes 2816 | tf_op jit(solution)/shard_map/reduce_or | solution.py:691
  1.7 0.1 reshape.29
  1.8 0.1 select_reduce_fusion.1
  2.0 0.1 broadcast_in_dim.48
  2.0 0.6 pad.19.slots_ref
  2.6 0.1 add.63
  2.7 1.4 %select_reduce_fusion = s32[2,16,16]{2,1,0:T(8,128)S(1)} fusion(s32[2,128]{1,0:T(2,128)S(1)} %broadcast_in_dim.48, s32[2,16,16]{2,1,0:T(8,128)} %param.28), kind=kLoop, calls=%fused_computation | loop fusion | flops 196096 | bytes 5120 | tf_op jit(solution)/shard_map/reduce_sum | solution.py:697
  4.2 1.3 %broadcast_multiply_fusion = (s32[2,16,16]{2,1,0:T(8,128)S(1)}, s32[2,16,16]{2,1,0:T(8,128)}) fusion(s32[2,16,16]{2,1,0:T(8,128)} %param.28, s32[2,16,16]{2,1,0:T(8,128)S(1)} %select_reduce_fusion, s32[]{:T(128)S(6)} %axis_index.15), kind=kLoop, calls=%fused_computation.17 | loop fusion | flops 14336 | bytes 8196 | tf_op jit(solution)/shard_map/mul | solution.py:705
  5.5 0.8 %copy.19 = bf16[128,64]{1,0:T(8,128)(2,1)S(1)} copy(bf16[128,64]{0,1:T(8,128)(2,1)} %param.23) | data formatting | bytes 32768 | tf_op args[7]
  6.3 0.6 %pad.16.sko_ref = bf16[128,128]{1,0:T(8,128)(2,1)} pad(bf16[128,64]{1,0:T(8,128)(2,1)S(1)} %copy.19, bf16[]{:T(256)} %constant.53.clone.1), padding=0_0x0_64 | pad | bytes 49154 | tf_op jit(solution)/shard_map/jit(_pad)/pad | solution.py:709
  7.0 0.8 %copy.20 = bf16[128,64]{1,0:T(8,128)(2,1)S(1)} copy(bf16[128,64]{0,1:T(8,128)(2,1)} %param.25) | data formatting | bytes 32768 | tf_op args[9]
  7.8 0.7 %pad.17.svo_ref = bf16[128,128]{1,0:T(8,128)(2,1)} pad(bf16[128,64]{1,0:T(8,128)(2,1)S(1)} %copy.20, bf16[]{:T(256)} %constant.53.clone.1), padding=0_0x64_0 | pad | bytes 49154 | tf_op jit(solution)/shard_map/jit(_pad)/pad | solution.py:710
  8.5 0.1 add.60
  8.6 0.1 add.61
  8.8 0.6 %broadcast_add_fusion.keypos_ref = s32[32,512]{1,0:T(8,128)} fusion(s32[32,512]{1,0:T(8,128)S(1)} %add.61, s32[512]{0:T(512)S(1)} %add.63), kind=kLoop, calls=%fused_computation.5 | loop fusion | flops 16384 | bytes 133120 | tf_op jit(solution)/shard_map/add | solution.py:705
  9.4 1.7 %pad.18.gate_ref = bf16[128,2048]{1,0:T(8,128)(2,1)} pad(bf16[16,2048]{1,0:T(8,128)(2,1)} %bitcast.7, bf16[]{:T(256)} %constant.53.clone.1), padding=0_112x0_0 | pad | bytes 589826 | tf_op jit(solution)/shard_map/jit(_pad)/pad | solution.py:708
  11.1 47.4 %layer.1 = bf16[128,2048]{1,0:T(8,128)(2,1)} custom-call(s32[32,16]{1,0:T(8,128)} %bitcast.6, bf16[512,2048]{1,0:T(8,128)(2,1)} %tokens_hbm.1, bf16[2048,512]{1,0:T(8,128)(2,1)} %wq_hbm.1, bf16[2048,128]{1,0:T(8,128)(2,1)} %wck_hbm.1, bf16[2048,128]{1,0:T(8,128)(2,1)} %wcv_hbm.1, bf16[2048,128]{1,0:T(8,128)(2,1)} %wsk_hbm.1, bf16[2048,128]{1,0:T(8,128)(2,1)} %wsv_hbm.1, ...), custom_call_target="tpu_custom_call" | custom-call | tf_op jit(solution)/shard_map/layer/pallas_call | solution.py:720
  58.5 1.9 %copy.22 = bf16[128,2048]{1,0:T(8,128)(2,1)} copy(bf16[128,2048]{1,0:T(8,128)(2,1)} %layer.1) | data formatting | bytes 1048576
  (5 shorter events, 0.0 us)

commit v2 on v1

--- a/solution.py
+++ b/solution.py
@@ -246,7 +246,8 @@
     n,
     groups,
     per_group,
-    loc_ref,
+    chosen_ref,
+    chosen_vec,
     tokens_hbm,
     wq_hbm,
     wck_hbm,
@@ -259,8 +260,6 @@
     svo_ref,
     gate_ref,
     wo_hbm,
-    slots_ref,
-    keypos_ref,
     turns_ref,
     bases_ref,
     sturns_ref,
@@ -272,6 +271,10 @@
     wki,
     wvi,
     wo,
+    wo_other,
+    slots_ref,
+    locs,
+    locmap,
     slotbuf,
     kvc,
     kvstage,
@@ -284,13 +287,11 @@
     qbuf,
     gates,
     gath,
+    compr,
     blended,
-    part_a,
+    blended_got,
     part_b,
-    part_c,
-    got_a,
     got_b,
-    got_c,
     load_sem,
     slot_send,
     slot_recv,
@@ -302,6 +303,7 @@
     halo_recv,
     rs_send,
     rs_recv,
+    loc_sem,
 ):
     me = lax.axis_index("kv")
     tp = lax.axis_index("tp")
@@ -340,8 +342,31 @@
         load(svi_hbm.at[0:half], wvi.at[:, 0:LANES]),
         load(svi_hbm.at[half : 2 * half], wvi.at[:, LANES : 2 * LANES]),
     ]
-    load_q = [load(wq_hbm, wq)]
-    load_o = [load(wo_hbm, wo)]
+
+    every = n * blocks
+    lane = lax.broadcasted_iota(jnp.int32, (blocks, every), 1)
+    query_block = me * blocks + lax.broadcasted_iota(jnp.int32, (blocks, 1), 0)
+    row8 = lax.broadcasted_iota(jnp.int32, (8, every), 0)
+    lane8 = lax.broadcasted_iota(jnp.int32, (8, every), 1)
+    present = jnp.zeros((8, every), jnp.int32)
+    for g in range(groups):
+        asked = chosen_vec[g]
+        asked = jnp.where(asked <= query_block, asked, -1)
+        hit = jnp.where(asked[:, 0:1] == lane, 1, 0)
+        for k in range(1, asked.shape[1]):
+            hit = jnp.where(asked[:, k : k + 1] == lane, 1, hit)
+        hit = jnp.max(hit, 0, keepdims=True)
+        present = jnp.where(row8 == g, hit, present)
+    slot = jnp.zeros((8, every), jnp.int32)
+    for s in range(1, blocks):
+        slot = slot + jnp.where(lane8 % blocks >= s, pltpu.roll(present, s, 1), 0)
+    slots_ref[...] = jnp.where(present > 0, slot, -1).astype(jnp.float32)
+    owner = lane8 // blocks
+    locs[...] = jnp.where(
+        owner == me,
+        n * CAP + lane8 % blocks,
+        jnp.where(owner < me, owner * CAP + jnp.minimum(slot, CAP - 1), n * CAP),
+    )
 
     sumbuf[...] = jnp.zeros_like(sumbuf)
     halo_in[...] = jnp.zeros_like(halo_in)
@@ -357,6 +382,9 @@
             barrier, inc=1, device_id={"tp": other}, device_id_type=pl.DeviceIdType.MESH
         )
     pl.semaphore_wait(barrier, n + 1)
+
+    loc_copy = pltpu.make_async_copy(locs, locmap, loc_sem)
+    loc_copy.start()
 
     def slot_copy(d, src_rank, dst_rank):
         return pltpu.make_async_remote_copy(
@@ -413,6 +441,11 @@
         @pl.when(me - d >= 0)
         def _(d=d):
             slot_copy(d, me, me - d).start()
+
+    load_q = [load(wq_hbm, wq)]
+    load_o = [load(wo_hbm, wo)]
+    weight_copy = rs_copy(0, wo_hbm, wo_other, partner)
+    weight_copy.start()
 
     base_cos = bases_ref[me, 0:1, :]
     base_sin = bases_ref[me, 1:2, :]
@@ -508,7 +541,8 @@
                 for k in range(step // BLK):
                     at = (first // BLK + k) * per_group * BLK + r * BLK
                     qbuf[g, at : at + BLK, :] = part[k * BLK : (k + 1) * BLK, :]
-    gates[...] = jax.nn.sigmoid(dot_nt(tok[...], gate_ref[...]))
+    gate_rows = jnp.concatenate([gate_ref[k].astype(jnp.float32) for k in range(2)], 0)
+    gates[...] = jax.nn.sigmoid(dot_nt(tok[...], gate_rows.astype(jnp.bfloat16)))
 
     @pl.when(me < n - 1)
     def _():
@@ -526,7 +560,10 @@
             )
             per.append(here[:, :LANES] + following)
         hidden.append(jax.nn.gelu(jnp.concatenate(per, 0)).astype(jnp.bfloat16))
-    summed = dot(hidden[0], sko_ref[...]) + dot(hidden[1], svo_ref[...])
+    none = jnp.zeros(sko_ref.shape, jnp.float32)
+    key_out = jnp.concatenate([sko_ref[...].astype(jnp.float32), none], 0).astype(jnp.bfloat16)
+    value_out = jnp.concatenate([none, svo_ref[...].astype(jnp.float32)], 0).astype(jnp.bfloat16)
+    summed = dot_nt(hidden[0], key_out) + dot_nt(hidden[1], value_out)
     low = low_half((summaries, LANES))
     sc = sturns_ref[0]
     ss = sturns_ref[1]
@@ -548,10 +585,9 @@
         @pl.when(me - d >= 0)
         def _(d=d):
             sum_copy(d, me - d, me).wait_recv()
-            kv_copy(d, me - d, me).wait_recv()
 
     total = n * summaries
-    listed = keypos_ref.shape[1]
+    listed = chosen_vec.shape[2]
     qrows = per_group * BLK
     in_block = lax.broadcasted_iota(jnp.int32, (qrows, 1), 0) % BLK
     ends = lax.broadcasted_iota(jnp.int32, (1, total), 1) * CMP_STRIDE + CMP_LEN - 1
@@ -564,72 +600,109 @@
         total_weight = jnp.sum(weights, -1, keepdims=True)
         return dot(weights.astype(jnp.bfloat16), pairs), total_weight
 
-    def attend(target):
+    def gate_column(b, first):
+        gate = gates[pl.ds(pl.multiple_of(b * BLK, BLK), BLK), :]
+        return jnp.concatenate(
+            [gate[:, first + r : first + r + 1] for r in range(per_group)], 0
+        )
+
+    def compressed_block(b, _):
+        pos = me * rows + b * BLK + in_block
+        at = pl.ds(pl.multiple_of(b * qrows, qrows), qrows)
+        for g in range(groups):
+            mixed, weight = mix(qbuf[g, at, :], sumbuf[g], ends <= pos)
+            inverse = gate_column(b, g * per_group) / jnp.maximum(weight, 1.0)
+            compr[g, at, :] = mixed * inverse
+        return 0
+
+    lax.fori_loop(0, blocks, compressed_block, 0)
+
+    loc_copy.wait()
+    for d in range(1, n):
+
+        @pl.when(me - d >= 0)
+        def _(d=d):
+            kv_copy(d, me - d, me).wait_recv()
+
+    tile_lane = lax.broadcasted_iota(jnp.int32, (1, LANES), 1)
+
+    def attend(target, first, count, dst):
         def block(i, _):
-            b = target * per_chunk + i
+            b = target * per_chunk + first + i
             pos = me * rows + b * BLK + in_block
-            gate = gates[pl.ds(pl.multiple_of(b * BLK, BLK), BLK), :]
+            at = pl.ds(pl.multiple_of(b * qrows, qrows), qrows)
             for g in range(groups):
-                q = qbuf[g, pl.ds(pl.multiple_of(b * qrows, qrows), qrows), :]
-                for k in range(listed // BLK):
-                    where = loc_ref[g * blocks + b, k]
-                    gath[g, k * BLK : (k + 1) * BLK, :] = kvbuf[g, where]
-                compressed, csum = mix(q, sumbuf[g], ends <= pos)
-                key_positions = keypos_ref[pl.ds(g * blocks + b, 1), :]
-                selected, ssum = mix(q, gath[g], key_positions <= pos)
-                cinv = 1.0 / jnp.maximum(csum, 1.0)
-                sinv = 1.0 / ssum
-                heads_out = []
-                for r in range(per_group):
-                    part = slice(r * BLK, (r + 1) * BLK)
-                    h = g * per_group + r
-                    heads_out.append(
-                        compressed[part] * (cinv[part] * gate[:, h : h + 1])
-                        + selected[part] * (sinv[part] * gate[:, heads + h : heads + h + 1])
-                    )
+                key_tiles = []
+                for k in range(0, listed, LANES // BLK):
+                    which = jnp.zeros((1, LANES), jnp.int32)
+                    for e in range(LANES // BLK):
+                        chosen = chosen_ref[g, b, k + e]
+                        where = locmap[g, chosen]
+                        gath[g, (k + e) * BLK : (k + e + 1) * BLK, :] = kvbuf[g, where]
+                        which = jnp.where(tile_lane // BLK == e, chosen, which)
+                    key_tiles.append(which * BLK + tile_lane % BLK)
+                key_positions = jnp.concatenate(key_tiles, 1)
+                mixed, weight = mix(qbuf[g, at, :], gath[g], key_positions <= pos)
+                inverse = gate_column(b, heads + g * per_group) / weight
+                both = compr[g, at, :] + mixed * inverse
                 for r in range(0, per_group, 2):
                     joined = jnp.where(
-                        low_half((BLK, LANES)), pltpu.roll(heads_out[r], HD, 1), heads_out[r + 1]
+                        low_half((BLK, LANES)),
+                        pltpu.roll(both[r * BLK : (r + 1) * BLK], HD, 1),
+                        both[(r + 1) * BLK : (r + 2) * BLK],
                     )
-                    at = (g * per_group + r) * HD
-                    blended[pl.ds(pl.multiple_of(i * BLK, BLK), BLK), at : at + LANES] = (
+                    column = (g * per_group + r) * HD
+                    dst[pl.ds(pl.multiple_of(i * BLK, BLK), BLK), column : column + LANES] = (
                         joined.astype(jnp.bfloat16)
                     )
             return 0
 
-        lax.fori_loop(0, per_chunk, block, 0)
+        lax.fori_loop(0, count, block, 0)
 
     tile = 512
     columns = wo.shape[1]
 
-    def project(dst, added):
+    def project(dst, mine, theirs, added):
         for at in range(0, columns, tile):
-            piece = dot(blended[...], wo[:, at : at + tile])
+            piece = dot(mine[...], wo[:, at : at + tile])
+            piece = piece + dot(theirs[...], wo_other[:, at : at + tile])
             for other in added:
                 piece = piece + other[:, at : at + tile].astype(jnp.float32)
             dst[:, at : at + tile] = piece.astype(jnp.bfloat16)
 
-    attend(diagonal)
-    for copy in load_o:
-        copy.wait()
-    project(part_a, [])
-    send_a = rs_copy(0, part_a, got_a, partner)
-    send_a.start()
-    attend(across)
-    send_a.wait_recv()
-    project(part_b, [got_a])
-    send_b = rs_copy(1, part_b, got_b, across)
-    send_b.start()
-    attend(partner)
-    project(part_c, [])
-    send_c = rs_copy(2, part_c, got_c, partner)
-    send_c.start()
-    attend(tp)
-    send_c.wait_recv()
-    send_b.wait_recv()
-    project(out_ref, [got_c, got_b])
-
-    for copy in (send_a, send_b, send_c):
+    part = per_chunk // 2
+    part_rows = part * BLK
+    sends = []
+    arrivals = []
+    for h in range(2):
+        span = pl.ds(h * part_rows, part_rows)
+        attend(diagonal, h * part, part, blended.at[0, span])
+        send = rs_copy(1 + h, blended.at[0, span], blended_got.at[0, span], partner)
+        send.start()
+        sends.append(send)
+        attend(across, h * part, part, blended.at[1, span])
+        if h == 0:
+            for copy in load_o:
+                copy.wait()
+            weight_copy.wait_recv()
+        send.wait_recv()
+        project(part_b.at[span], blended.at[1, span], blended_got.at[0, span], [])
+        send = rs_copy(3 + h, part_b.at[span], got_b.at[span], across)
+        send.start()
+        sends.append(send)
+        arrivals.append(send)
+    attend(partner, 0, per_chunk, blended.at[2])
+    send = rs_copy(5, blended.at[2], blended_got.at[1], partner)
+    send.start()
+    sends.append(send)
+    attend(tp, 0, per_chunk, blended.at[3])
+    send.wait_recv()
+    for arrival in arrivals:
+        arrival.wait_recv()
+    project(out_ref, blended.at[3], blended_got.at[1], [got_b])
+
+    sends.append(weight_copy)
+    for copy in sends:
         copy.wait_send()
     for d in range(1, n):
 
@@ -683,31 +756,8 @@
     heads = groups * per_group
     blocks = rows // BLK
     listed = chosen.shape[2]
-    me = lax.axis_index("kv")
-    query_block = me * blocks + jnp.arange(blocks, dtype=jnp.int32)
     every = n * blocks
-    hit = chosen[..., None] == jnp.arange(every, dtype=jnp.int32)
-    counted = hit & (chosen <= query_block[None, :, None])[..., None]
-    present = jnp.any(counted, axis=(1, 2))
-    by_shard = present.reshape(groups, n, blocks).astype(jnp.int32)
-    earlier = jnp.arange(blocks)[:, None] < jnp.arange(blocks)[None, :]
-    slot = jnp.sum(jnp.where(earlier, by_shard[..., None], 0), axis=2).reshape(groups, every)
-    slots = jnp.where(present, slot, -1).astype(jnp.float32)
-    slots = jnp.pad(slots, ((0, 8 - groups), (0, 0)), constant_values=-1.0)
-    chosen_slot = jnp.sum(jnp.where(hit, slot[:, None, None, :], 0), -1)
-    owner = chosen // blocks
-    loc = jnp.where(
-        owner == me,
-        n * CAP + chosen % blocks,
-        jnp.where(owner < me, owner * CAP + jnp.minimum(chosen_slot, CAP - 1), n * CAP),
-    ).reshape(groups * blocks, listed)
-    keypos = (
-        chosen[..., None] * BLK + jnp.arange(BLK, dtype=jnp.int32)
-    ).reshape(groups * blocks, listed * BLK)
-    gate = gate_weight.transpose(0, 2, 1).reshape(2 * heads, depth)
-    gate = jnp.pad(gate, ((0, LANES - 2 * heads), (0, 0)))
-    sko = jnp.pad(sko, ((0, 0), (0, HD)))
-    svo = jnp.pad(svo, ((0, 0), (HD, 0)))
+    gate = gate_weight.transpose(0, 2, 1)
     local, bases, ends = rotary_constants(rows, n)
     chunk = rows // 4
     bf = jnp.bfloat16
@@ -720,11 +770,11 @@
     return pl.pallas_call(
         functools.partial(layer_kernel, n, groups, per_group),
         out_shape=jax.ShapeDtypeStruct((chunk, wo.shape[1]), bf),
-        in_specs=[pl.BlockSpec(memory_space=pltpu.SMEM)]
+        in_specs=[pl.BlockSpec(memory_space=pltpu.SMEM), vmem]
         + [hbm] * 8
         + [vmem] * 3
         + [hbm]
-        + [vmem] * 5,
+        + [vmem] * 3,
         out_specs=vmem,
         scratch_shapes=[
             pltpu.VMEM((rows, depth), bf),
@@ -734,6 +784,10 @@
             pltpu.VMEM((CMP_STRIDE * HD, 2 * LANES), bf),
             pltpu.VMEM((CMP_STRIDE * HD, 2 * LANES), bf),
             pltpu.VMEM(wo.shape, bf),
+            pltpu.VMEM(wo.shape, bf),
+            pltpu.VMEM((8, every), jnp.float32),
+            pltpu.VMEM((8, every), jnp.int32),
+            pltpu.SMEM((8, every), jnp.int32),
             pltpu.VMEM((n, 8, every), jnp.float32),
             pltpu.VMEM((groups, rows, LANES), bf),
             pltpu.VMEM((n, groups, CAP, BLK, LANES), bf),
@@ -744,13 +798,11 @@
             pltpu.VMEM((groups, summaries, LANES), bf),
             pltpu.VMEM((groups, n * summaries, LANES), bf),
             pltpu.VMEM((groups, rows * per_group, LANES), bf),
-            pltpu.VMEM((rows, LANES), jnp.float32),
+            pltpu.VMEM((rows, 2 * heads), jnp.float32),
             pltpu.VMEM((groups, listed * BLK, LANES), bf),
-            pltpu.VMEM((chunk, heads * HD), bf),
-            part,
-            part,
-            part,
-            part,
+            pltpu.VMEM((groups, rows * per_group, LANES), jnp.float32),
+            pltpu.VMEM((4, chunk, heads * HD), bf),
+            pltpu.VMEM((2, chunk, heads * HD), bf),
             part,
             part,
             dma((11,)),
@@ -762,14 +814,15 @@
             dma((n,)),
             dma(()),
             dma(()),
-            dma((3,)),
-            dma((3,)),
+            dma((6,)),
+            dma((6,)),
+            dma(()),
         ],
         compiler_params=pltpu.CompilerParams(
             collective_id=0, has_side_effects=True, vmem_limit_bytes=60 * 1024 * 1024
         ),
         name="layer",
-    )(loc, tokens, wq, wck, wcv, wsk, wsv, ski, svi, sko, svo, gate, wo, slots, keypos, local, bases, ends)
+    )(chosen, chosen, tokens, wq, wck, wcv, wsk, wsv, ski, svi, sko.T, svo.T, gate, wo, local, bases, ends)
 
 
 def solution(mesh):

time: 61.1 us -> 55.3 us (0.905)
  Pallas kernels: 47.4 us -> 53.2 us
  local copies, waits for them, and re-layouts: 7.64 us -> 1.88 us
  other arithmetic: 5.27 us -> 0 us
    pallas_call x1, Pallas kernels: 47.4 us -> 53.2 us  [fused(): pl.pallas_call(functools.partial(layer_kernel, n, groups, per_group), out...]
    pad x4 -> x0, local copies, waits for them, and re-layouts: 3.6 us -> none  [the longest x1 1.68 us: fused(): gate = jnp.pad(gate, ((0, LANES - 2 * heads), (0, 0)))]
    unnamed x3 -> x1, local copies, waits for them, and re-layouts: 3.53 us -> 1.88 us
    reduce_sum x2 -> x0, other arithmetic: 1.55 us -> none  [the longest x1 1.43 us: fused(): chosen_slot = jnp.sum(jnp.where(hit, slot[:, None, None, :], 0), -1)]
    mul x1 -> x0, other arithmetic: 1.34 us -> none  [fused(): chosen[..., None] * BLK + jnp.arange(BLK, dtype=jnp.int32)]
    reduce_or x1 -> x0, other arithmetic: 0.93 us -> none  [fused(): present = jnp.any(counted, axis=(1, 2))]
    le x1 -> x0, other arithmetic: 0.79 us -> none  [fused(): counted = hit & (chosen <= query_block[None, :, None])[..., None]]
    add x2 -> x0, other arithmetic: 0.63 us -> none  [the longest x1 0.63 us: fused(): chosen[..., None] * BLK + jnp.arange(BLK, dtype=jnp.int32)]
where the time goes in v2:
time: 55.3 us; the launch traced here: 55.1 us
  Pallas kernels  53.2 us (96%)
  local copies, waits for them, and re-layouts  1.88 us (3%)
    pallas_call x1, Pallas kernels, fused(): pl.pallas_call(functools.partial(layer_kernel, n, groups, per_group), out...  53.2 us
    unnamed x1, local copies, waits for them, and re-layouts  1.88 us

profile of v2, /device:TPU:26, one launch (start us, length us, event | category | flops | bytes accessed | tf_op | source)
XLA Modules:
  0.0 55.1 jit_solution(8663941274321843884)
XLA Ops:
  0.0 53.2 %layer.1 = bf16[128,2048]{1,0:T(8,128)(2,1)} custom-call(s32[2,16,16]{2,1,0:T(8,128)} %chosen_vec.1, s32[2,16,16]{2,1,0:T(8,128)} %chosen_vec.1, bf16[512,2048]{1,0:T(8,128)(2,1)} %tokens_hbm.1, bf16[2048,512]{1,0:T(8,128)(2,1)} %wq_hbm.1, bf16[2048,128]{1,0:T(8,128)(2,1)} %wck_hbm.1, bf16[2048,128]{1,0:T(8,128)(2,1)} %wcv_hbm.1, bf16[2048,128]{1,0:T(8,128)(2,1)} %wsk_hbm.1, ...), custom_call_target="tpu_custom_call" | custom-call | tf_op jit(solution)/shard_map/layer/pallas_call | solution.py:770
  53.3 1.9 %copy.18 = bf16[128,2048]{1,0:T(8,128)(2,1)} copy(bf16[128,2048]{1,0:T(8,128)(2,1)} %layer.1) | data formatting | bytes 1048576

commit v3 on v2

--- a/solution.py
+++ b/solution.py
@@ -596,7 +596,7 @@
     def mix(q, pairs, visible):
         scores = jnp.where(visible, dot_nt(q, pairs), NEGATIVE_FILL)
         largest = jnp.max(scores, -1, keepdims=True)
-        weights = jnp.where(visible, jnp.exp(scores - largest), 0.0)
+        weights = jnp.exp(scores - largest)
         total_weight = jnp.sum(weights, -1, keepdims=True)
         return dot(weights.astype(jnp.bfloat16), pairs), total_weight
 
@@ -612,10 +612,10 @@
         for g in range(groups):
             mixed, weight = mix(qbuf[g, at, :], sumbuf[g], ends <= pos)
             inverse = gate_column(b, g * per_group) / jnp.maximum(weight, 1.0)
-            compr[g, at, :] = mixed * inverse
+            compr[g, at, :] = jnp.where(pos >= CMP_LEN - 1, mixed * inverse, 0.0)
         return 0
 
-    lax.fori_loop(0, blocks, compressed_block, 0)
+    lax.fori_loop(0, blocks, compressed_block, 0, unroll=2)
 
     loc_copy.wait()
     for d in range(1, n):
@@ -627,7 +627,12 @@
     tile_lane = lax.broadcasted_iota(jnp.int32, (1, LANES), 1)
 
     def attend(target, first, count, dst):
-        def block(i, _):
+        def blocks_pair(i, _):
+            block(2 * i, 0)
+            block(2 * i + 1, 1)
+            return 0
+
+        def block(i, slot):
             b = target * per_chunk + first + i
             pos = me * rows + b * BLK + in_block
             at = pl.ds(pl.multiple_of(b * qrows, qrows), qrows)
@@ -638,11 +643,11 @@
                     for e in range(LANES // BLK):
                         chosen = chosen_ref[g, b, k + e]
                         where = locmap[g, chosen]
-                        gath[g, (k + e) * BLK : (k + e + 1) * BLK, :] = kvbuf[g, where]
+                        gath[slot, g, (k + e) * BLK : (k + e + 1) * BLK, :] = kvbuf[g, where]
                         which = jnp.where(tile_lane // BLK == e, chosen, which)
                     key_tiles.append(which * BLK + tile_lane % BLK)
                 key_positions = jnp.concatenate(key_tiles, 1)
-                mixed, weight = mix(qbuf[g, at, :], gath[g], key_positions <= pos)
+                mixed, weight = mix(qbuf[g, at, :], gath[slot, g], key_positions <= pos)
                 inverse = gate_column(b, heads + g * per_group) / weight
                 both = compr[g, at, :] + mixed * inverse
                 for r in range(0, per_group, 2):
@@ -655,9 +660,11 @@
                     dst[pl.ds(pl.multiple_of(i * BLK, BLK), BLK), column : column + LANES] = (
                         joined.astype(jnp.bfloat16)
                     )
-            return 0
-
-        lax.fori_loop(0, count, block, 0)
+
+        if count == 2:
+            blocks_pair(0, 0)
+        else:
+            lax.fori_loop(0, count // 2, blocks_pair, 0)
 
     tile = 512
     columns = wo.shape[1]
@@ -799,7 +806,7 @@
             pltpu.VMEM((groups, n * summaries, LANES), bf),
             pltpu.VMEM((groups, rows * per_group, LANES), bf),
             pltpu.VMEM((rows, 2 * heads), jnp.float32),
-            pltpu.VMEM((groups, listed * BLK, LANES), bf),
+            pltpu.VMEM((2, groups, listed * BLK, LANES), bf),
             pltpu.VMEM((groups, rows * per_group, LANES), jnp.float32),
             pltpu.VMEM((4, chunk, heads * HD), bf),
             pltpu.VMEM((2, chunk, heads * HD), bf),
@@ -829,7 +836,8 @@
     n = mesh.shape["kv"]
 
     def one_device(*args):
-        fits = args[2].shape[1] == LANES and mesh.shape["tp"] == 4
+        whole_blocks = args[0].shape[0] % (16 * BLK) == 0
+        fits = args[2].shape[1] == LANES and mesh.shape["tp"] == 4 and whole_blocks
         return fused(n, *args) if fits else on_device(*args)
 
     return jax.shard_map(

time: 55.3 us -> 50.6 us (0.915)
  Pallas kernels: 53.2 us -> 48.6 us
    pallas_call x1, Pallas kernels: 53.2 us -> 48.6 us  [fused(): pl.pallas_call(functools.partial(layer_kernel, n, groups, per_group), out...]
where the time goes in v3:
time: 50.6 us; the launch traced here: 50.5 us
  Pallas kernels  48.6 us (96%)
  local copies, waits for them, and re-layouts  1.88 us (4%)
    pallas_call x1, Pallas kernels, fused(): pl.pallas_call(functools.partial(layer_kernel, n, groups, per_group), out...  48.6 us
    unnamed x1, local copies, waits for them, and re-layouts  1.88 us

profile of v3, /device:TPU:26, one launch (start us, length us, event | category | flops | bytes accessed | tf_op | source)
XLA Modules:
  0.0 50.5 jit_solution(4439044918978766330)
XLA Ops:
  0.0 48.6 %layer.1 = bf16[128,2048]{1,0:T(8,128)(2,1)} custom-call(s32[2,16,16]{2,1,0:T(8,128)} %chosen_vec.1, s32[2,16,16]{2,1,0:T(8,128)} %chosen_vec.1, bf16[512,2048]{1,0:T(8,128)(2,1)} %tokens_hbm.1, bf16[2048,512]{1,0:T(8,128)(2,1)} %wq_hbm.1, bf16[2048,128]{1,0:T(8,128)(2,1)} %wck_hbm.1, bf16[2048,128]{1,0:T(8,128)(2,1)} %wcv_hbm.1, bf16[2048,128]{1,0:T(8,128)(2,1)} %wsk_hbm.1, ...), custom_call_target="tpu_custom_call" | custom-call | tf_op jit(solution)/shard_map/layer/pallas_call | solution.py:777
  48.6 1.9 %copy.18 = bf16[128,2048]{1,0:T(8,128)(2,1)} copy(bf16[128,2048]{1,0:T(8,128)(2,1)} %layer.1) | data formatting | bytes 1048576
